TPU v7x, 32 devices: a whole 2x2x4 slice. The times are simulated.
32 devices in a mesh: fs: 8 (over z, y), tp: 4 (over x, core).
Axes of the slice: x: 2, y: 2, z: 4, core: 2. Of those that a mesh axis runs over, the one named last changes fastest.
Arguments:
- tokens: bfloat16 [8192, 2048], P('fs'), may hold values from -6 to 6
- norm_gain: float32 [2048], replicated, may hold values from 0.1 to 1.9
- gate_weight: bfloat16 [2048, 4096], P('fs', 'tp'), may hold values from -0.125 to 0.125
- up_weight: bfloat16 [2048, 4096], P('fs', 'tp'), may hold values from -0.125 to 0.125
- down_weight: bfloat16 [4096, 2048], P('tp', 'fs'), may hold values from -2 to 2
- out_gain: float32 [2048], P('tp'), may hold values from 0.1 to 1.9
Outputs:
- result: bfloat16 [8192, 2048], P('fs', 'tp')
All inputs are finite; a program needn't handle non-finite values.
Results may differ from a plain program's by a relative error of at most 0.014.
Values may be sent and summed in bfloat16 or wider, within the bound.
No kernel may reach another device: no remote copies, remote signals or barrier semaphores. Data moves between devices by JAX's collectives and lax.ppermute only.
A program may use at most 64 MiB of HBM per device.

v0:
```python
import jax
import jax.numpy as jnp
from jax import lax
from jax.sharding import PartitionSpec as P

EPSILON = 1e-06


def body(tokens, norm_gain, gate_weight, up_weight, down_weight, out_gain):
    values = tokens.astype(jnp.float32)
    normed = (
        values * lax.rsqrt(jnp.mean(values * values, axis=1, keepdims=True) + EPSILON) * norm_gain
    ).astype(jnp.bfloat16)
    gate_all, up_all = (
        lax.all_gather(gate_weight, "fs", axis=0, tiled=True),
        lax.all_gather(up_weight, "fs", axis=0, tiled=True),
    )
    gate_proj = jnp.dot(normed, gate_all, preferred_element_type=jnp.float32)
    up_proj = jnp.dot(normed, up_all, preferred_element_type=jnp.float32)
    hidden = (jax.nn.silu(gate_proj) * up_proj).astype(jnp.bfloat16)
    partial_value = jnp.dot(
        hidden,
        lax.all_gather(down_weight, "fs", axis=1, tiled=True),
        preferred_element_type=jnp.float32,
    )
    own_width = out_gain.shape[0]
    own_columns = lax.psum_scatter(
        partial_value.astype(jnp.bfloat16), "tp", scatter_dimension=1, tiled=True
    ).astype(jnp.float32)
    squares = lax.psum(jnp.sum(own_columns * own_columns, axis=1), "tp")
    mean_square = squares / (own_width * lax.axis_size("tp"))
    scaled = own_columns * lax.rsqrt(mean_square + EPSILON)[:, None] * out_gain[None, :]
    return scaled.astype(jnp.bfloat16)


def solution(mesh):
    return jax.shard_map(
        body,
        mesh=mesh,
        in_specs=(P("fs", None), P(), P("fs", "tp"), P("fs", "tp"), P("tp", "fs"), P("tp")),
        out_specs=P("fs", "tp"),
        check_vma=False,
    )
```

profile of v0, /device:TPU:0, one launch (start us, length us, event | category | flops | bytes accessed | tf_op | source)
XLA Modules:
  0.0 308.2 jit_solution(11775894596299125198)
XLA Ops:
  6.5 0.0 copy-start.1
  6.5 0.0 all-gather.4.cloned.1.call-start
  6.5 0.7 all-gather.4.cloned.1.call-update
  7.3 0.0 all-gather.6.cloned.1.call-start
  7.3 0.7 all-gather.6.cloned.1.call-update
  8.0 0.0 all-gather.8.cloned.1.call-start
  8.1 0.7 all-gather.8.cloned.1.call-update
  8.7 0.0 reduce-scatter.2.cloned.1.call-start
  8.8 3.1 fusion
  11.9 73.1 %all-gather.4.cloned.1.call-done = bf16[2048,1024]{1,0:T(8,128)(2,1)} async-done(((bf16[256,1024]{1,0:T(8,128)(2,1)}), bf16[2048,1024]{1,0:T(8,128)(2,1)}) %all-gather.4.cloned.1.call-update) | async-done | bytes 4194320 | tf_op jit(solution)/shard_map/all_gather | solution.py:15
  85.0 0.0 copy-done.1
  85.0 10.0 %fusion.7 = f32[1024,1024]{1,0:T(8,128)} fusion(bf16[2048,1024]{1,0:T(8,128)(2,1)} %all-gather.4.cloned.1.call-done, bf16[1024,2048]{1,0:T(8,128)(2,1)} %param.6, f32[2048]{0:T(1024)S(1)} %copy-done.1, f32[1024]{0:T(1024)S(1)} %add_rsqrt_fusion.1), kind=kOutput, calls=%fused_computation.12 | convolution fusion | flops 4303355904 | bytes 12595200 | tf_op jit(solution)/shard_map/dot_general | solution.py:18
  95.0 63.5 %all-gather.6.cloned.1.call-done = bf16[2048,1024]{1,0:T(8,128)(2,1)} async-done(((bf16[256,1024]{1,0:T(8,128)(2,1)}), bf16[2048,1024]{1,0:T(8,128)(2,1)}) %all-gather.6.cloned.1.call-update) | async-done | bytes 4194320 | tf_op jit(solution)/shard_map/all_gather | solution.py:16
  158.5 75.3 %all-gather.8.cloned.1.call-done = bf16[1024,2048]{1,0:T(8,128)(2,1)} async-done(((bf16[1024,256]{1,0:T(8,128)(2,1)}), bf16[1024,2048]{1,0:T(8,128)(2,1)}) %all-gather.8.cloned.1.call-update) | async-done | bytes 4194320 | tf_op jit(solution)/shard_map/all_gather | solution.py:23
  233.7 15.3 %convolution_convert_fusion = bf16[1024,2048]{1,0:T(8,128)(2,1)} fusion(bf16[1024,2048]{1,0:T(8,128)(2,1)} %all-gather.8.cloned.1.call-done, f32[1024,1024]{1,0:T(8,128)} %fusion.7, bf16[2048,1024]{1,0:T(8,128)(2,1)} %all-gather.6.cloned.1.call-done, bf16[1024,2048]{1,0:T(8,128)(2,1)} %param.6, f32[2048]{0:T(1024)S(1)} %copy-done.1, ...), kind=kOutput, calls=%fused_computation.6 | convolution fusion | flops 8606711808 | bytes 20983808 | tf_op jit(solution)/shard_map/dot_general | solution.py:21
  249.1 0.0 copy-start
  249.1 0.0 reduce-scatter.2.cloned.1.call-update
  249.1 42.7 %reduce-scatter.2.cloned.1.call-done = bf16[1024,512]{1,0:T(8,128)(2,1)} async-done(((bf16[1024,2048]{1,0:T(8,128)(2,1)}), bf16[1024,512]{1,0:T(8,128)(2,1)}) %reduce-scatter.2.cloned.1.call-update) | async-done | bytes 1048592 | tf_op jit(solution)/shard_map/reduce_scatter | solution.py:27
  291.9 1.5 fusion.3
  293.4 5.8 %psum.7 = f32[1024]{0:T(1024)S(1)} all-reduce(f32[1024]{0:T(1024)S(1)} %fusion.3), channel_id=1, replica_groups=mesh['fs'=8,'tp'=4] {'tp'}, use_global_device_ids=true, to_apply=%region_3.4 | all-reduce | flops 1024 | bytes 8192 | tf_op jit(solution)/shard_map/psum | solution.py:30
  299.1 0.0 copy-done
  299.1 2.5 fusion.5
  (2 shorter events, 0.0 us)
Async XLA Ops:
  6.5 78.5 %copy-start.1 = (f32[2048]{0:T(1024)S(1)}, f32[2048]{0:T(1024)}, u32[]{:S(2)}) copy-start(f32[2048]{0:T(1024)} %param.7) | copy-start | bytes 24580
  6.5 78.5 %all-gather.4.cloned.1.call-start = ((), (), s32[]{:S(2)}) async-start(), calls=%async_computation.1 | async-start | bytes 4718592 | tf_op jit(solution)/shard_map/all_gather | solution.py:15
  7.3 151.2 %all-gather.6.cloned.1.call-start = ((), (), s32[]{:S(2)}) async-start(), calls=%async_computation.2 | async-start | bytes 4718592 | tf_op jit(solution)/shard_map/all_gather | solution.py:16
  8.0 225.7 %all-gather.8.cloned.1.call-start = ((), (), s32[]{:S(2)}) async-start(), calls=%async_computation.3 | async-start | bytes 4718592 | tf_op jit(solution)/shard_map/all_gather | solution.py:23
  8.7 283.1 %reduce-scatter.2.cloned.1.call-start = ((), (), s32[]{:S(2)}) async-start(), calls=%async_computation.4 | async-start | bytes 5242880 | tf_op jit(solution)/shard_map/reduce_scatter | solution.py:27
  249.1 50.0 %copy-start = (f32[512]{0:T(512)S(1)}, f32[512]{0:T(512)}, u32[]{:S(2)}) copy-start(f32[512]{0:T(512)} %param.11) | copy-start | bytes 6148
Sparse Core Ops, SparseCore 0:
  9.5 75.5 all-gather.3
  87.1 71.3 all-gather.5
  160.5 73.1 all-gather.7
  249.2 42.5 reduce-scatter.1
where the time goes:
time: 308 us
  waiting for transfers between devices  257 us (83%)
  matrix products  25.3 us (8%)
  between operations  13.1 us (4%)
  other arithmetic  7.09 us (2%)
  blocking collectives  5.77 us (2%)
    all_gather x1, waiting for transfers between devices, body(): lax.all_gather(down_weight, 'fs', axis=1, tiled=True)  75.3 us
    all_gather x1, waiting for transfers between devices, body(): lax.all_gather(gate_weight, 'fs', axis=0, tiled=True)  73.1 us
    all_gather x1, waiting for transfers between devices, body(): lax.all_gather(up_weight, 'fs', axis=0, tiled=True)  63.5 us
    reduce_scatter x1, waiting for transfers between devices, body(): lax.psum_scatter(partial_value.astype(jnp.bfloat16), 'tp', scatter_dimens...  42.7 us
    dot_general x1, matrix products, body(): jnp.dot(hidden, lax.all_gather(down_weight, 'fs', axis=1, tiled=True), pr...  15.3 us
    dot_general x1, matrix products, body(): gate_proj = jnp.dot(normed, gate_all, preferred_element_type=jnp.float32)  9.96 us
  transfers between devices with their start and end apart: 4, of which 4 were waited for; matrix products, arithmetic and copies ran while one was open for 4% of the time, Pallas kernels for 0%

commit v1 on v0

--- a/solution.py
+++ b/solution.py
@@ -6,13 +6,24 @@
 EPSILON = 1e-06
 
 
+def collect(value, axis, dim):
+    ways = lax.axis_size(axis)
+    pieces = [value]
+    for far in range(1, ways):
+        pieces.append(
+            lax.ppermute(pieces[far - 1], axis, [(d, (d - 1) % ways) for d in range(ways)])
+        )
+    line = jnp.concatenate(pieces, axis=dim)
+    return jnp.roll(line, lax.axis_index(axis) * value.shape[dim], axis=dim)
+
+
 def body(tokens, norm_gain, gate_weight, up_weight, down_weight, out_gain):
     values = tokens.astype(jnp.float32)
     normed = (
         values * lax.rsqrt(jnp.mean(values * values, axis=1, keepdims=True) + EPSILON) * norm_gain
     ).astype(jnp.bfloat16)
     gate_all, up_all = (
-        lax.all_gather(gate_weight, "fs", axis=0, tiled=True),
+        collect(gate_weight, "fs", 0),
         lax.all_gather(up_weight, "fs", axis=0, tiled=True),
     )
     gate_proj = jnp.dot(normed, gate_all, preferred_element_type=jnp.float32)

time: 308 us -> 288 us (0.935)
  waiting for transfers between devices: 257 us -> 182 us
  starting transfers between devices: 0.12 us -> 37.3 us
  local copies, waits for them, and re-layouts: 0.01 us -> 16.5 us
    ppermute x0 -> x7, waiting for transfers between devices: none -> 106 us  [collect(): lax.ppermute(pieces[far - 1], axis, [(d, (d - 1) % ways) for d in range(w...]
    all_gather x1 -> x0, waiting for transfers between devices: 73.1 us -> none  [body(): lax.all_gather(gate_weight, 'fs', axis=0, tiled=True)]
    all_gather x1, waiting for transfers between devices: 63.5 us -> 0.01 us  [body(): lax.all_gather(up_weight, 'fs', axis=0, tiled=True)]
    all_gather x1, waiting for transfers between devices: 75.3 us -> 31.7 us  [body(): lax.all_gather(down_weight, 'fs', axis=1, tiled=True)]
    ppermute x0 -> x7, starting transfers between devices: none -> 37.2 us  [collect(): lax.ppermute(pieces[far - 1], axis, [(d, (d - 1) % ways) for d in range(w...]
    unnamed x4 -> x21, local copies, waits for them, and re-layouts: 0.01 us -> 15.6 us
  transfers between devices with their start and end apart: 4 -> 10, of which waited for: 4 -> 9; matrix products, arithmetic and copies ran while one was open for 4% -> 10% of each run, Pallas kernels for 0% -> 0%
where the time goes in v1:
time: 288 us
  waiting for transfers between devices  182 us (63%)
  starting transfers between devices  37.3 us (13%)
  matrix products  25.7 us (9%)
  local copies, waits for them, and re-layouts  16.5 us (6%)
  between operations  13.2 us (5%)
  other arithmetic  7.09 us (2%)
  blocking collectives  5.77 us (2%)
    ppermute x7, waiting for transfers between devices, collect(): lax.ppermute(pieces[far - 1], axis, [(d, (d - 1) % ways) for d in range(w...  106 us
    reduce_scatter x1, waiting for transfers between devices, body(): lax.psum_scatter(partial_value.astype(jnp.bfloat16), 'tp', scatter_dimens...  42.8 us
    ppermute x7, starting transfers between devices, collect(): lax.ppermute(pieces[far - 1], axis, [(d, (d - 1) % ways) for d in range(w...  37.2 us
    all_gather x1, waiting for transfers between devices, body(): lax.all_gather(down_weight, 'fs', axis=1, tiled=True)  31.7 us
    dot_general x1, matrix products, body(): jnp.dot(hidden, lax.all_gather(down_weight, 'fs', axis=1, tiled=True), pr...  15.6 us
    unnamed x21, local copies, waits for them, and re-layouts  15.6 us
    dot_general x1, matrix products, body(): up_proj = jnp.dot(normed, up_all, preferred_element_type=jnp.float32)  10.1 us
    psum x1, blocking collectives, body(): squares = lax.psum(jnp.sum(own_columns * own_columns, axis=1), 'tp')  5.77 us
  transfers between devices with their start and end apart: 10, of which 9 were waited for; matrix products, arithmetic and copies ran while one was open for 10% of the time, Pallas kernels for 0%

profile of v1, /device:TPU:0, one launch (start us, length us, event | category | flops | bytes accessed | tf_op | source)
XLA Modules:
  0.0 287.7 jit_solution(12533305621783459778)
XLA Ops:
  6.5 0.0 all-gather.3.cloned.1.call-start
  6.5 0.7 all-gather.3.cloned.1.call-update
  7.3 0.0 all-gather.5.cloned.1.call-start
  7.3 0.7 all-gather.5.cloned.1.call-update
  8.0 0.0 reduce-scatter.2.cloned.1.call-start
  8.1 6.1 %collective-permute-start = (bf16[256,1024]{1,0:T(8,128)(2,1)}, bf16[256,1024]{1,0:T(8,128)(2,1)S(1)}, u32[]{:S(2)}, u32[]{:S(2)}) collective-permute-start(bf16[256,1024]{1,0:T(8,128)(2,1)} %param.8), channel_id=1, source_target_pairs={{0,28},{4,0},{8,4},{12,8},{16,12},{20,16},{24,20},{28,24},{1,29},{... | collective-permute-start | bytes 1572872 | tf_op jit(solution)/shard_map/ppermute | solution.py:14
  14.1 17.0 %collective-permute-done = bf16[256,1024]{1,0:T(8,128)(2,1)S(1)} collective-permute-done((bf16[256,1024]{1,0:T(8,128)(2,1)}, bf16[256,1024]{1,0:T(8,128)(2,1)S(1)}, u32[]{:S(2)}, u32[]{:S(2)}) %collective-permute-start) | collective-permute-done | bytes 524320 | tf_op jit(solution)/shard_map/ppermute | solution.py:14
  31.2 5.1 %collective-permute-start.1 = (bf16[256,1024]{1,0:T(8,128)(2,1)S(1)}, bf16[256,1024]{1,0:T(8,128)(2,1)S(1)}, u32[]{:S(2)}, u32[]{:S(2)}) collective-permute-start(bf16[256,1024]{1,0:T(8,128)(2,1)S(1)} %collective-permute-done), channel_id=1, source_target_pairs={{0,28},{4,0},{8,4},{12,8},{16,12},{20,16},{24,20},{28,24},{1,29},{... | collective-permute-start | bytes 1572872 | tf_op jit(solution)/shard_map/ppermute | solution.py:14
  36.3 17.4 %collective-permute-done.1 = bf16[256,1024]{1,0:T(8,128)(2,1)S(1)} collective-permute-done((bf16[256,1024]{1,0:T(8,128)(2,1)S(1)}, bf16[256,1024]{1,0:T(8,128)(2,1)S(1)}, u32[]{:S(2)}, u32[]{:S(2)}) %collective-permute-start.1) | collective-permute-done | bytes 524320 | tf_op jit(solution)/shard_map/ppermute | solution.py:14
  53.6 5.2 %collective-permute-start.2 = (bf16[256,1024]{1,0:T(8,128)(2,1)S(1)}, bf16[256,1024]{1,0:T(8,128)(2,1)S(1)}, u32[]{:S(2)}, u32[]{:S(2)}) collective-permute-start(bf16[256,1024]{1,0:T(8,128)(2,1)S(1)} %collective-permute-done.1), channel_id=1, source_target_pairs={{0,28},{4,0},{8,4},{12,8},{16,12},{20,16},{24,20},{28,24},{1,29},{... | collective-permute-start | bytes 1572872 | tf_op jit(solution)/shard_map/ppermute | solution.py:14
  58.8 21.4 %collective-permute-done.2 = bf16[256,1024]{1,0:T(8,128)(2,1)S(1)} collective-permute-done((bf16[256,1024]{1,0:T(8,128)(2,1)S(1)}, bf16[256,1024]{1,0:T(8,128)(2,1)S(1)}, u32[]{:S(2)}, u32[]{:S(2)}) %collective-permute-start.2) | collective-permute-done | bytes 524320 | tf_op jit(solution)/shard_map/ppermute | solution.py:14
  80.2 5.2 %collective-permute-start.3 = (bf16[256,1024]{1,0:T(8,128)(2,1)S(1)}, bf16[256,1024]{1,0:T(8,128)(2,1)S(1)}, u32[]{:S(2)}, u32[]{:S(2)}) collective-permute-start(bf16[256,1024]{1,0:T(8,128)(2,1)S(1)} %collective-permute-done.2), channel_id=1, source_target_pairs={{0,28},{4,0},{8,4},{12,8},{16,12},{20,16},{24,20},{28,24},{1,29},{... | collective-permute-start | bytes 1572872 | tf_op jit(solution)/shard_map/ppermute | solution.py:14
  85.4 21.7 %collective-permute-done.3 = bf16[256,1024]{1,0:T(8,128)(2,1)S(1)} collective-permute-done((bf16[256,1024]{1,0:T(8,128)(2,1)S(1)}, bf16[256,1024]{1,0:T(8,128)(2,1)S(1)}, u32[]{:S(2)}, u32[]{:S(2)}) %collective-permute-start.3) | collective-permute-done | bytes 524320 | tf_op jit(solution)/shard_map/ppermute | solution.py:14
  107.2 5.2 %collective-permute-start.4 = (bf16[256,1024]{1,0:T(8,128)(2,1)S(1)}, bf16[256,1024]{1,0:T(8,128)(2,1)S(1)}, u32[]{:S(2)}, u32[]{:S(2)}) collective-permute-start(bf16[256,1024]{1,0:T(8,128)(2,1)S(1)} %collective-permute-done.3), channel_id=1, source_target_pairs={{0,28},{4,0},{8,4},{12,8},{16,12},{20,16},{24,20},{28,24},{1,29},{... | collective-permute-start | bytes 1572872 | tf_op jit(solution)/shard_map/ppermute | solution.py:14
  112.4 12.7 %collective-permute-done.4 = bf16[256,1024]{1,0:T(8,128)(2,1)S(1)} collective-permute-done((bf16[256,1024]{1,0:T(8,128)(2,1)S(1)}, bf16[256,1024]{1,0:T(8,128)(2,1)S(1)}, u32[]{:S(2)}, u32[]{:S(2)}) %collective-permute-start.4) | collective-permute-done | bytes 524320 | tf_op jit(solution)/shard_map/ppermute | solution.py:14
  125.1 5.2 %collective-permute-start.5 = (bf16[256,1024]{1,0:T(8,128)(2,1)S(1)}, bf16[256,1024]{1,0:T(8,128)(2,1)}, u32[]{:S(2)}, u32[]{:S(2)}) collective-permute-start(bf16[256,1024]{1,0:T(8,128)(2,1)S(1)} %collective-permute-done.4), channel_id=1, source_target_pairs={{0,28},{4,0},{8,4},{12,8},{16,12},{20,16},{24,20},{28,24},{1,29},{... | collective-permute-start | bytes 1572872 | tf_op jit(solution)/shard_map/ppermute | solution.py:14
  130.3 3.1 %fusion = f32[1024]{0:T(1024)S(1)} fusion(bf16[1024,2048]{1,0:T(8,128)(2,1)} %param.6), kind=kLoop, calls=%fused_computation.2 | loop fusion | flops 6290432 | bytes 4198400 | tf_op jit(solution)/shard_map/reduce_sum | solution.py:23
  133.4 0.0 copy-start.2
  133.4 1.9 constant_dynamic-update-slice_fusion.15
  135.3 0.8 constant_dynamic-update-slice_fusion.14
  136.1 8.3 %collective-permute-done.5 = bf16[256,1024]{1,0:T(8,128)(2,1)} collective-permute-done((bf16[256,1024]{1,0:T(8,128)(2,1)S(1)}, bf16[256,1024]{1,0:T(8,128)(2,1)}, u32[]{:S(2)}, u32[]{:S(2)}) %collective-permute-start.5) | collective-permute-done | bytes 524320 | tf_op jit(solution)/shard_map/ppermute | solution.py:14
  144.4 5.3 %collective-permute-start.6 = (bf16[256,1024]{1,0:T(8,128)(2,1)}, bf16[256,1024]{1,0:T(8,128)(2,1)S(1)}, u32[]{:S(2)}, u32[]{:S(2)}) collective-permute-start(bf16[256,1024]{1,0:T(8,128)(2,1)} %collective-permute-done.5), channel_id=1, source_target_pairs={{0,28},{4,0},{8,4},{12,8},{16,12},{20,16},{24,20},{28,24},{1,29},{... | collective-permute-start | bytes 1572872 | tf_op jit(solution)/shard_map/ppermute | solution.py:14
  149.7 0.8 constant_dynamic-update-slice_fusion.13
  150.6 0.8 constant_dynamic-update-slice_fusion.12
  151.4 0.8 constant_dynamic-update-slice_fusion.11
  152.2 0.8 constant_dynamic-update-slice_fusion.10
  153.1 1.9 constant_dynamic-update-slice_fusion.9
  154.9 7.7 %collective-permute-done.6 = bf16[256,1024]{1,0:T(8,128)(2,1)S(1)} collective-permute-done((bf16[256,1024]{1,0:T(8,128)(2,1)}, bf16[256,1024]{1,0:T(8,128)(2,1)S(1)}, u32[]{:S(2)}, u32[]{:S(2)}) %collective-permute-start.6) | collective-permute-done | bytes 524320 | tf_op jit(solution)/shard_map/ppermute | solution.py:14
  162.6 0.8 constant_dynamic-update-slice_fusion.8
  163.4 0.0 copy-done
  163.4 0.8 constant_dynamic-update-slice_fusion.7
  164.2 0.8 constant_dynamic-update-slice_fusion.6
  165.1 0.8 constant_dynamic-update-slice_fusion.5
  165.9 0.8 constant_dynamic-update-slice_fusion.4
  166.7 0.8 constant_dynamic-update-slice_fusion.3
  167.6 0.8 constant_dynamic-update-slice_fusion.2
  168.4 1.9 constant_dynamic-update-slice_fusion.1
  170.3 0.9 constant_dynamic-update-slice_fusion
  171.1 0.0 copy-done.2
  171.1 10.1 %fusion.13 = f32[1024,1024]{1,0:T(8,128)} fusion(bf16[2048,1024]{1,0:T(8,128)(2,1)} %all-gather.3.cloned.1.call-done, bf16[1024,2048]{1,0:T(8,128)(2,1)} %param.6, f32[2048]{0:T(1024)S(1)} %copy-done.2, f32[1024]{0:T(1024)S(1)} %add_rsqrt_fusion.1), kind=kOutput, calls=%fused_computation.15 | convolution fusion | flops 4303355904 | bytes 12595200 | tf_op jit(solution)/shard_map/dot_general | solution.py:30
  181.2 31.7 %all-gather.5.cloned.1.call-done = bf16[1024,2048]{1,0:T(8,128)(2,1)} async-done(((bf16[1024,256]{1,0:T(8,128)(2,1)}), bf16[1024,2048]{1,0:T(8,128)(2,1)}) %all-gather.5.cloned.1.call-update) | async-done | bytes 4194320 | tf_op jit(solution)/shard_map/all_gather | solution.py:34
  213.0 15.6 %convolution_convert_fusion = bf16[1024,2048]{1,0:T(8,128)(2,1)} fusion(bf16[1024,2048]{1,0:T(8,128)(2,1)} %all-gather.5.cloned.1.call-done, f32[1024,1024]{1,0:T(8,128)} %fusion.13, bf16[4096,1024]{1,0:T(8,128)(2,1)} %constant_dynamic-update-slice_fusion, s32[]{:T(128)S(6)} %select_n.14, bf16[1024,2048]{1,0:T(8,128)(2,1)} %param.6, f32[2048]{0:T(1024)S(1)} %copy-done.2, ...), kind=kOutput, calls=%fused_computation.8 | convolution fusion | flops 8606711808 | bytes 20983812 | tf_op jit(solution)/shard_map/dot_general | solution.py:32
  228.6 0.0 reduce-scatter.2.cloned.1.call-update
  228.6 42.8 %reduce-scatter.2.cloned.1.call-done = bf16[1024,512]{1,0:T(8,128)(2,1)} async-done(((bf16[1024,2048]{1,0:T(8,128)(2,1)}), bf16[1024,512]{1,0:T(8,128)(2,1)}) %reduce-scatter.2.cloned.1.call-update) | async-done | bytes 1048592 | tf_op jit(solution)/shard_map/reduce_scatter | solution.py:38
  271.4 1.5 fusion.9
  272.9 5.8 %psum.7 = f32[1024]{0:T(1024)S(1)} all-reduce(f32[1024]{0:T(1024)S(1)} %fusion.9), channel_id=1, replica_groups=mesh['fs'=8,'tp'=4] {'tp'}, use_global_device_ids=true, to_apply=%region_3.4 | all-reduce | flops 1024 | bytes 8192 | tf_op jit(solution)/shard_map/psum | solution.py:41
  278.7 0.0 copy-done.1
  278.7 2.5 fusion.11
  (5 shorter events, 0.0 us)
Async XLA Ops:
  6.5 156.9 %copy-start = (bf16[256,1024]{1,0:T(8,128)(2,1)S(1)}, bf16[256,1024]{1,0:T(8,128)(2,1)}, u32[]{:S(2)}) copy-start(bf16[256,1024]{1,0:T(8,128)(2,1)} %param.8) | copy-start | bytes 1572868
  6.5 164.6 %all-gather.3.cloned.1.call-start = ((), (), s32[]{:S(2)}) async-start(), calls=%async_computation.1 | async-start | bytes 4718592 | tf_op jit(solution)/shard_map/all_gather | solution.py:27
  7.3 205.7 %all-gather.5.cloned.1.call-start = ((), (), s32[]{:S(2)}) async-start(), calls=%async_computation.2 | async-start | bytes 4718592 | tf_op jit(solution)/shard_map/all_gather | solution.py:34
  8.0 263.4 %reduce-scatter.2.cloned.1.call-start = ((), (), s32[]{:S(2)}) async-start(), calls=%async_computation.3 | async-start | bytes 5242880 | tf_op jit(solution)/shard_map/reduce_scatter | solution.py:38
  8.1 23.1 %collective-permute-start = (bf16[256,1024]{1,0:T(8,128)(2,1)}, bf16[256,1024]{1,0:T(8,128)(2,1)S(1)}, u32[]{:S(2)}, u32[]{:S(2)}) collective-permute-start(bf16[256,1024]{1,0:T(8,128)(2,1)} %param.8), channel_id=1, source_target_pairs={{0,28},{4,0},{8,4},{12,8},{16,12},{20,16},{24,20},{28,24},{1,29},{... | collective-permute-start | bytes 1572872 | tf_op jit(solution)/shard_map/ppermute | solution.py:14
  31.2 22.4 %collective-permute-start.1 = (bf16[256,1024]{1,0:T(8,128)(2,1)S(1)}, bf16[256,1024]{1,0:T(8,128)(2,1)S(1)}, u32[]{:S(2)}, u32[]{:S(2)}) collective-permute-start(bf16[256,1024]{1,0:T(8,128)(2,1)S(1)} %collective-permute-done), channel_id=1, source_target_pairs={{0,28},{4,0},{8,4},{12,8},{16,12},{20,16},{24,20},{28,24},{1,29},{... | collective-permute-start | bytes 1572872 | tf_op jit(solution)/shard_map/ppermute | solution.py:14
  53.6 26.6 %collective-permute-start.2 = (bf16[256,1024]{1,0:T(8,128)(2,1)S(1)}, bf16[256,1024]{1,0:T(8,128)(2,1)S(1)}, u32[]{:S(2)}, u32[]{:S(2)}) collective-permute-start(bf16[256,1024]{1,0:T(8,128)(2,1)S(1)} %collective-permute-done.1), channel_id=1, source_target_pairs={{0,28},{4,0},{8,4},{12,8},{16,12},{20,16},{24,20},{28,24},{1,29},{... | collective-permute-start | bytes 1572872 | tf_op jit(solution)/shard_map/ppermute | solution.py:14
  80.2 26.9 %collective-permute-start.3 = (bf16[256,1024]{1,0:T(8,128)(2,1)S(1)}, bf16[256,1024]{1,0:T(8,128)(2,1)S(1)}, u32[]{:S(2)}, u32[]{:S(2)}) collective-permute-start(bf16[256,1024]{1,0:T(8,128)(2,1)S(1)} %collective-permute-done.2), channel_id=1, source_target_pairs={{0,28},{4,0},{8,4},{12,8},{16,12},{20,16},{24,20},{28,24},{1,29},{... | collective-permute-start | bytes 1572872 | tf_op jit(solution)/shard_map/ppermute | solution.py:14
  107.2 17.9 %collective-permute-start.4 = (bf16[256,1024]{1,0:T(8,128)(2,1)S(1)}, bf16[256,1024]{1,0:T(8,128)(2,1)S(1)}, u32[]{:S(2)}, u32[]{:S(2)}) collective-permute-start(bf16[256,1024]{1,0:T(8,128)(2,1)S(1)} %collective-permute-done.3), channel_id=1, source_target_pairs={{0,28},{4,0},{8,4},{12,8},{16,12},{20,16},{24,20},{28,24},{1,29},{... | collective-permute-start | bytes 1572872 | tf_op jit(solution)/shard_map/ppermute | solution.py:14
  125.1 19.3 %collective-permute-start.5 = (bf16[256,1024]{1,0:T(8,128)(2,1)S(1)}, bf16[256,1024]{1,0:T(8,128)(2,1)}, u32[]{:S(2)}, u32[]{:S(2)}) collective-permute-start(bf16[256,1024]{1,0:T(8,128)(2,1)S(1)} %collective-permute-done.4), channel_id=1, source_target_pairs={{0,28},{4,0},{8,4},{12,8},{16,12},{20,16},{24,20},{28,24},{1,29},{... | collective-permute-start | bytes 1572872 | tf_op jit(solution)/shard_map/ppermute | solution.py:14
  133.4 37.8 %copy-start.2 = (f32[2048]{0:T(1024)S(1)}, f32[2048]{0:T(1024)}, u32[]{:S(2)}) copy-start(f32[2048]{0:T(1024)} %param.7) | copy-start | bytes 24580
  144.4 18.2 %collective-permute-start.6 = (bf16[256,1024]{1,0:T(8,128)(2,1)}, bf16[256,1024]{1,0:T(8,128)(2,1)S(1)}, u32[]{:S(2)}, u32[]{:S(2)}) collective-permute-start(bf16[256,1024]{1,0:T(8,128)(2,1)} %collective-permute-done.5), channel_id=1, source_target_pairs={{0,28},{4,0},{8,4},{12,8},{16,12},{20,16},{24,20},{28,24},{1,29},{... | collective-permute-start | bytes 1572872 | tf_op jit(solution)/shard_map/ppermute | solution.py:14
  181.2 97.4 %copy-start.1 = (f32[512]{0:T(512)S(1)}, f32[512]{0:T(512)}, u32[]{:S(2)}) copy-start(f32[512]{0:T(512)} %param.11) | copy-start | bytes 6148
Sparse Core Ops, SparseCore 0:
  9.5 110.5 all-gather.2
  122.1 90.8 all-gather.4
  228.7 42.5 reduce-scatter.1
